TPU v7x, 32 devices: a whole 2x2x4 slice. The times are simulated.
32 devices in a mesh: ep: 32 (over z, y, x, core).
Axes of the slice: x: 2, y: 2, z: 4, core: 2. Of those that a mesh axis runs over, the one named last changes fastest.
Arguments:
- tokens: bfloat16 [768, 2048], P('ep'), may hold values from -6 to 6
- lengths: int32 [768], P('ep'), may hold values from 2 to 1024
- latent_cache: bfloat16 [768, 1024, 256], P('ep'), may hold values from -500 to 500
- rotary_cache: bfloat16 [768, 1024, 32], P('ep'), may hold values from -6 to 6
- route_ids: int32 [768, 6], P('ep'), may hold values from 0 to 31, all different within a row; in each aligned block of 24 rows (0 to 23, 24 to 47, ...) at most 12 rows name the same one
- route_scores: float32 [768, 6], P('ep'), may hold values from 0.05 to 1
- attn_gain: bfloat16 [2048], replicated, may hold values from 0.099609375 to 1.8984375
- w_query_down: bfloat16 [2048, 256], replicated, may hold values from -0.125 to 0.125
- query_gain: bfloat16 [256], replicated, may hold values from 0.099609375 to 1.8984375
- w_query_nope: bfloat16 [256, 2048], replicated, may hold values from -0.375 to 0.375
- w_query_rope: bfloat16 [256, 1024], replicated, may hold values from -0.375 to 0.375
- w_key_absorb: bfloat16 [32, 64, 256], replicated, may hold values from -0.75 to 0.75
- latent_gain: bfloat16 [256], replicated, may hold values from 0.099609375 to 1.8984375
- w_latent_down: bfloat16 [2048, 256], replicated, may hold values from -0.125 to 0.125
- w_rotary_key: bfloat16 [2048, 32], replicated, may hold values from -0.125 to 0.125
- w_value_up: bfloat16 [32, 256, 64], replicated, may hold values from -0.375 to 0.375
- w_output: bfloat16 [2048, 2048], P(None, 'ep'), may hold values from -0.125 to 0.125
- ffn_gain: bfloat16 [2048], replicated, may hold values from 0.099609375 to 1.8984375
- expert_gate: bfloat16 [32, 2048, 512], P('ep'), may hold values from -0.125 to 0.125
- expert_up: bfloat16 [32, 2048, 512], P('ep'), may hold values from -0.125 to 0.125
- expert_down: bfloat16 [32, 512, 2048], P('ep'), may hold values from -0.25 to 0.25
- shared_gate: bfloat16 [2048, 256], replicated, may hold values from -0.125 to 0.125
- shared_up: bfloat16 [2048, 256], replicated, may hold values from -0.125 to 0.125
- shared_down: bfloat16 [256, 2048], replicated, may hold values from -0.375 to 0.375
Outputs:
- mixed: bfloat16 [768, 2048], P('ep')
- latent_new: bfloat16 [768, 256], P('ep')
- rotary_new: bfloat16 [768, 32], P('ep')
Inputs may be any that keep to these rules, and one draw needn't show every extreme that they name: `route_ids`: within the rows of one device no expert is named by more than 12 rows, a bound that some block reaches; each row names 6 different experts. `lengths`: cache positions at or past a sequence's length are not read.
All inputs are finite; a program needn't handle non-finite values.
Results may differ from a plain program's by a relative error of at most 0.025.
Values may be sent and summed in bfloat16 or wider, within the bound.
A program may use at most 128 MiB of HBM per device.

v0:
```python
import jax
import jax.numpy as jnp
from jax import lax
from jax.sharding import PartitionSpec as P

EPSILON = 1e-06
THETA = 10000.0
ROUTED_SCALE = 2.5


def rms_scale(values, gain):
    squares = jnp.mean(values * values, axis=-1, keepdims=True)
    return values * lax.rsqrt(squares + EPSILON) * gain.astype(jnp.float32)


def rotate(values, positions):
    half = values.shape[-1] // 2
    freqs = 1.0 / THETA ** (jnp.arange(half, dtype=jnp.float32) * 2.0 / values.shape[-1])
    angles = positions.astype(jnp.float32)[:, None] * freqs[None, :]
    if values.ndim == 3:
        angles = angles[:, None, :]
    cosine, sine = (jnp.cos(angles), jnp.sin(angles))
    first, second = (values[..., :half], values[..., half:])
    return jnp.concatenate(
        [first * cosine - second * sine, second * cosine + first * sine], axis=-1
    )


def shards(
    tokens,
    lengths,
    latent_cache,
    rotary_cache,
    route_ids,
    route_scores,
    attn_gain,
    w_query_down,
    query_gain,
    w_query_nope,
    w_query_rope,
    w_key_absorb,
    latent_gain,
    w_latent_down,
    w_rotary_key,
    w_value_up,
    w_output,
    ffn_gain,
    expert_gate,
    expert_up,
    expert_down,
    shared_gate,
    shared_up,
    shared_down,
):
    f32 = jnp.float32
    bf16 = jnp.bfloat16
    rows, model = tokens.shape
    heads, nope, latent = w_key_absorb.shape
    rotary = w_rotary_key.shape[1]
    top = route_ids.shape[1]
    normed = rms_scale(tokens.astype(f32), attn_gain).astype(bf16)
    query_low = rms_scale(
        jnp.dot(normed, w_query_down, preferred_element_type=f32), query_gain
    ).astype(bf16)
    query_nope = (
        jnp.dot(query_low, w_query_nope, preferred_element_type=f32)
        .astype(bf16)
        .reshape(rows, heads, nope)
    )
    query_rot = jnp.dot(query_low, w_query_rope, preferred_element_type=f32).reshape(
        rows, heads, rotary
    )
    query_rot = rotate(query_rot, lengths).astype(bf16)
    query_lat = jnp.einsum(
        "thn,hnl->thl", query_nope, w_key_absorb, preferred_element_type=f32
    ).astype(bf16)
    latent_new = rms_scale(
        jnp.dot(normed, w_latent_down, preferred_element_type=f32), latent_gain
    ).astype(bf16)
    rotary_new = rotate(jnp.dot(normed, w_rotary_key, preferred_element_type=f32), lengths).astype(
        bf16
    )
    scale = (nope + rotary) ** (-0.5)
    scores = (
        jnp.einsum("thl,tkl->thk", query_lat, latent_cache, preferred_element_type=f32)
        + jnp.einsum("thr,tkr->thk", query_rot, rotary_cache, preferred_element_type=f32)
    ) * scale
    live = jnp.arange(latent_cache.shape[1], dtype=jnp.int32)[None, :] < lengths[:, None]
    scores = jnp.where(live[:, None, :], scores, -jnp.inf)
    own = (
        jnp.einsum("thl,tl->th", query_lat, latent_new, preferred_element_type=f32)
        + jnp.einsum("thr,tr->th", query_rot, rotary_new, preferred_element_type=f32)
    ) * scale
    highest = jnp.maximum(jnp.max(scores, axis=-1), own)
    weights = jnp.exp(scores - highest[..., None])
    own_weight = jnp.exp(own - highest)
    total = jnp.sum(weights, axis=-1) + own_weight
    probs = (weights / total[..., None]).astype(bf16)
    own_prob = (own_weight / total).astype(bf16)
    out_lat = jnp.einsum("thk,tkl->thl", probs, latent_cache, preferred_element_type=f32)
    out_lat = (
        out_lat + own_prob.astype(f32)[..., None] * latent_new.astype(f32)[:, None, :]
    ).astype(bf16)
    values = jnp.einsum("thl,hlv->thv", out_lat, w_value_up, preferred_element_type=f32).astype(
        bf16
    )
    values = values.reshape(rows, model)
    attended = jnp.dot(
        values, lax.all_gather(w_output, "ep", axis=1, tiled=True), preferred_element_type=f32
    ).astype(bf16)
    residual = (tokens.astype(f32) + attended.astype(f32)).astype(bf16)
    ffn_in = rms_scale(residual.astype(f32), ffn_gain).astype(bf16)
    devices = lax.axis_size("ep")
    local_experts = expert_gate.shape[0]
    experts = devices * local_experts
    capacity = max(2, rows * top * 8 // (3 * experts))
    flat_ids = route_ids.reshape(-1)
    hits = (flat_ids[:, None] == jnp.arange(experts, dtype=jnp.int32)[None, :]).astype(jnp.int32)
    earlier = jnp.cumsum(hits, axis=0) - hits
    slot = jnp.sum(earlier * hits, axis=1)
    target = flat_ids * capacity + slot
    slot_range = jnp.arange(experts * capacity, dtype=jnp.int32)
    per_token = jnp.any(
        slot_range[:, None, None] == target.reshape(rows, top)[None, :, :], axis=2
    ).astype(bf16)
    per_pair = (target[:, None] == slot_range[None, :]).astype(bf16)
    outgoing = (
        jnp.dot(per_token, ffn_in, preferred_element_type=f32)
        .astype(bf16)
        .reshape(experts, capacity, model)
    )
    arrived = lax.all_to_all(outgoing, "ep", split_axis=0, concat_axis=0, tiled=True)
    count = arrived.shape[1]
    grouped = arrived.reshape(devices, local_experts, count, model)
    gate = jnp.einsum("sjcd,jdf->sjcf", grouped, expert_gate, preferred_element_type=f32)
    upward = jnp.einsum("sjcd,jdf->sjcf", grouped, expert_up, preferred_element_type=f32)
    hidden = (jax.nn.silu(gate) * upward).astype(bf16)
    result = jnp.einsum("sjcf,jfd->sjcd", hidden, expert_down, preferred_element_type=f32).astype(
        bf16
    )
    returned = lax.all_to_all(
        result.reshape(devices * local_experts, count, model),
        "ep",
        split_axis=0,
        concat_axis=0,
        tiled=True,
    )
    picked = jnp.dot(
        per_pair, returned.reshape(experts * capacity, model), preferred_element_type=f32
    )
    route_weight = ROUTED_SCALE * route_scores / jnp.sum(route_scores, axis=1, keepdims=True)
    routed = jnp.sum(picked.reshape(rows, top, model) * route_weight[:, :, None], axis=1)
    gate_shared = jnp.dot(ffn_in, shared_gate, preferred_element_type=f32)
    up_shared = jnp.dot(ffn_in, shared_up, preferred_element_type=f32)
    hidden_shared = (jax.nn.silu(gate_shared) * up_shared).astype(bf16)
    shared_out = jnp.dot(hidden_shared, shared_down, preferred_element_type=f32)
    mixed = (residual.astype(f32) + routed + shared_out).astype(bf16)
    return (mixed, latent_new, rotary_new)


def solution(mesh):
    return jax.shard_map(
        shards,
        mesh=mesh,
        in_specs=(
            P("ep", None),
            P("ep"),
            P("ep", None, None),
            P("ep", None, None),
            P("ep", None),
            P("ep", None),
            P(),
            P(),
            P(),
            P(),
            P(),
            P(),
            P(),
            P(),
            P(),
            P(),
            P(None, "ep"),
            P(),
            P("ep", None, None),
            P("ep", None, None),
            P("ep", None, None),
            P(),
            P(),
            P(),
        ),
        out_specs=(P("ep", None), P("ep", None), P("ep", None)),
        check_vma=False,
    )
```

profile of v0, /device:TPU:0, one launch (start us, length us, event | category | flops | bytes accessed | tf_op | source)
XLA Modules:
  0.0 232.9 jit_solution(12893498353833350144)
XLA Ops:
  7.3 0.7 all-gather.2.cloned.1.call-update
  8.0 0.7 convert_element_type.102
  8.6 0.7 convert_element_type.104
  9.3 1.0 fusion.55
  10.3 1.7 multiply_reduce_fusion.2
  12.0 1.3 fusion.77
  13.5 1.5 convolution_convert_fusion.2
  15.0 0.9 reshape.206
  16.4 1.6 multiply_reduce_fusion.1
  19.5 8.8 %fusion.50 = f32[24,32,1024]{2,1,0:T(8,128)S(1)} fusion(bf16[24,1024,256]{2,1,0:T(8,128)(2,1)} %param.26, bf16[24,32,256]{2,0,1:T(8,128)(2,1)S(1)} %fusion.32), kind=kOutput, calls=%fused_computation.50 | convolution fusion | flops 402653184 | bytes 16121856 | tf_op jit(solution)/shard_map/thl,tkl->thk/dot_general | solution.py:85
  28.3 2.6 %fusion.87 = (f32[24,32]{1,0:T(8,128)S(1)}, f32[24,32,1024]{2,1,0:T(8,128)S(1)}) fusion(f32[24,32,1024]{2,1,0:T(8,128)S(1)} %fusion.50, bf16[24,1024,32]{1,2,0:T(8,128)(2,1)} %param.27, bf16[24,32,16]{2,1,0:T(8,128)(2,1)S(1)} %get-tuple-element.6, bf16[24,32,16]{2,1,0:T(8,128)(2,1)S(1)} %get-tuple-element.5, pred[24,1024]{1,0:T(8,128)(4,1)S(1)} %iota_compare_fusion.2), kind=kOutput, calls=%fused_computation.118 | convolution fusion | flops 53574912 | bytes 7941120 | tf_op jit(solution)/shard_map/thr,tkr->thk/dot_general | solution.py:86
  30.9 0.7 fusion
  31.6 2.1 fusion.28
  33.7 0.5 fusion.33
  34.7 0.6 reduce-window.6
  35.9 54.8 %all-gather.2.cloned.1.call-done = bf16[2048,2048]{0,1:T(8,128)(2,1)} async-done(((bf16[2048,64]{0,1:T(8,128)(2,1)}), bf16[2048,2048]{0,1:T(8,128)(2,1)}) %all-gather.2.cloned.1.call-update) | async-done | bytes 8388624 | tf_op jit(solution)/shard_map/all_gather | solution.py:109
  90.7 5.8 %multiply_reduce_fusion = (f32[24]{0:T(128)S(1)}, f32[24,2048]{1,0:T(8,128)S(1)}) fusion(bf16[24,2048]{1,0:T(8,128)(2,1)S(1)} %reshape.208, bf16[2048,2048]{0,1:T(8,128)(2,1)} %all-gather.2.cloned.1.call-done, bf16[24,2048]{1,0:T(8,128)(2,1)S(1)} %copy-done.2), kind=kOutput, calls=%fused_computation.64 | convolution fusion | flops 201719776 | bytes 8781920 | tf_op jit(solution)/shard_map/dot_general | solution.py:108
  96.5 1.8 convolution_convert_fusion
  98.3 3.6 %reshape.211 = bf16[32,12,2048]{2,1,0:T(8,128)(2,1)} reshape(bf16[384,2048]{1,0:T(8,128)(2,1)} %convolution_convert_fusion) | data formatting | bytes 3145728 | tf_op jit(solution)/shard_map/reshape | solution.py:130
  101.9 51.9 %all_to_all.10 = bf16[32,12,2048]{2,1,0:T(8,128)(2,1)S(1)} all-to-all(bf16[32,12,2048]{2,1,0:T(8,128)(2,1)} %reshape.211), channel_id=1, replica_groups=mesh['ep'=32] {'ep'}, dimensions={0} | all-to-all | bytes 3145728 | tf_op jit(solution)/shard_map/all_to_all | solution.py:132
  153.8 1.3 copy-done.1
  155.2 1.1 fusion.14
  156.3 5.5 %convolution_convert_fusion.1 = bf16[32,12,2048]{2,0,1:T(8,128)(2,1)} fusion(bf16[1,512,2048]{2,1,0:T(8,128)(2,1)S(1)} %copy-done, bf16[1,2048,512]{2,1,0:T(8,128)(2,1)} %param.43, bf16[32,12,2048]{2,1,0:T(8,128)(2,1)} %copy-done.1, f32[32,1,12,512]{3,0,2,1:T(8,128)S(1)} %fusion.14), kind=kOutput, calls=%fused_computation.4 | convolution fusion | flops 1612578816 | bytes 8126464 | tf_op jit(solution)/shard_map/sjcf,jfd->sjcd/dot_general | solution.py:138
  161.7 3.6 %copy.78 = bf16[32,12,2048]{2,1,0:T(8,128)(2,1)} copy(bf16[32,12,2048]{2,0,1:T(8,128)(2,1)} %convolution_convert_fusion.1) | data formatting | bytes 3145728 | tf_op jit(solution)/shard_map/convert_element_type | solution.py:138
  165.3 3.8 %all-to-all-start.1 = ((bf16[32,12,2048]{2,1,0:T(8,128)(2,1)}), bf16[32,12,2048]{2,1,0:T(8,128)(2,1)}, u32[]{:S(2)}, u32[]{:S(2)}) async-start(bf16[32,12,2048]{2,1,0:T(8,128)(2,1)} %copy.78), calls=%async_computation.1 | async-start | bytes 4194304 | tf_op jit(solution)/shard_map/all_to_all | solution.py:141
  169.1 0.7 pad_maximum_fusion.3
  169.8 0.6 multiply_divide_fusion
  170.4 0.9 fusion.79
  171.3 46.5 %all-to-all-done.1 = bf16[32,12,2048]{2,1,0:T(8,128)(2,1)} async-done(((bf16[32,12,2048]{2,1,0:T(8,128)(2,1)}), bf16[32,12,2048]{2,1,0:T(8,128)(2,1)}, u32[]{:S(2)}, u32[]{:S(2)}) %all-to-all-start.1) | async-done | bytes 1572896 | tf_op jit(solution)/shard_map/all_to_all | solution.py:141
  217.8 3.6 %reshape.225 = bf16[384,2048,1]{1,0,2:T(8,128)(2,1)} reshape(bf16[32,12,2048]{2,1,0:T(8,128)(2,1)} %all-to-all-done.1) | data formatting | bytes 3145728 | tf_op jit(solution)/shard_map/reshape | solution.py:149
  221.4 1.9 fusion.24
  223.4 2.7 %fusion.1 = bf16[24,2048]{1,0:T(8,128)(2,1)} fusion(bf16[256,2048]{1,0:T(8,128)(2,1)S(1)} %copy-done.6, bf16[2048,256]{1,0:T(8,128)(2,1)} %param.46, f32[24,2048]{1,0:T(8,128)S(1)} %get-tuple-element.20, f32[24,2048]{1,0:T(8,128)S(1)} %fusion.24, f32[24,256]{1,0:T(8,128)} %fusion.79, f32[2048]{0:T(1024)S(1)} %convert_element_type.124, f32[24]{0:T(128)S(1)} %add_rsqrt_fusion), kind=kOutput, calls=%fused_computation.8 | convolution fusion | flops 50663424 | bytes 2621536 | tf_op jit(solution)/shard_map/dot_general | solution.py:156
  (75 shorter events, 3.3 us)
Async XLA Ops:
  7.2 149.1 %copy-start = (bf16[1,512,2048]{2,1,0:T(8,128)(2,1)S(1)}, bf16[1,512,2048]{2,1,0:T(8,128)(2,1)}, u32[]{:S(2)}) copy-start(bf16[1,512,2048]{2,1,0:T(8,128)(2,1)} %param.44) | copy-start | bytes 6291460
  7.2 8.7 %copy-start.2 = (bf16[24,2048]{1,0:T(8,128)(2,1)S(1)}, bf16[24,2048]{1,0:T(8,128)(2,1)}, u32[]{:S(2)}) copy-start(bf16[24,2048]{1,0:T(8,128)(2,1)} %param.24) | copy-start | bytes 294916
  7.2 6.3 %copy-start.12 = (s32[24]{0:T(128)S(1)}, s32[24]{0:T(128)}, u32[]{:S(2)}) copy-start(s32[24]{0:T(128)} %param.25) | copy-start | bytes 292
  7.2 8.7 %copy-start.15 = (bf16[256]{0:T(256)(128)(2,1)S(1)}, bf16[256]{0:T(256)(128)(2,1)}, u32[]{:S(2)}) copy-start(bf16[256]{0:T(256)(128)(2,1)} %param.36) | copy-start | bytes 1540
  7.2 8.7 %copy-start.14 = (bf16[2048,32]{0,1:T(8,128)(2,1)S(1)}, bf16[2048,32]{0,1:T(8,128)(2,1)}, u32[]{:S(2)}) copy-start(bf16[2048,32]{0,1:T(8,128)(2,1)} %param.38) | copy-start | bytes 393220
  7.2 83.5 %all-gather.2.cloned.1.call-start = ((), (), s32[]{:S(2)}) async-start(), calls=%async_computation.2 | async-start | bytes 8650752 | tf_op jit(solution)/shard_map/all_gather | solution.py:109
  15.9 2.8 %copy-start.3 = (bf16[32,64,256]{2,1,0:T(8,128)(2,1)S(1)}, bf16[32,64,256]{2,1,0:T(8,128)(2,1)}, u32[]{:S(2)}) copy-start(bf16[32,64,256]{2,1,0:T(8,128)(2,1)} %param.35) | copy-start | bytes 3145732
  15.9 2.8 %copy-start.7 = (bf16[24,32,64]{2,1,0:T(8,128)(2,1)S(1)}, bf16[24,32,64]{2,1,0:T(8,128)(2,1)}, u32[]{:S(2)}) copy-start(bf16[24,32,64]{2,1,0:T(8,128)(2,1)} %reshape.206) | copy-start | bytes 294916
  18.7 0.6 copy-start.10
  19.5 12.1 %slice-start = ((s8[12582912]{0:T(1024)(128)(4,1)}), s8[4194304]{0:T(1024)(128)(4,1)S(1)}, s32[]{:S(2)}) async-start(s8[12582912]{0:T(1024)(128)(4,1)} %bitcast.91), calls=%async_computation.3 | async-start | bytes 8388608
  19.5 12.1 %slice-start.1 = ((s8[12582912]{0:T(1024)(128)(4,1)}), s8[4194304]{0:T(1024)(128)(4,1)S(1)}, s32[]{:S(2)}) async-start(s8[12582912]{0:T(1024)(128)(4,1)} %bitcast.91), calls=%async_computation.4 | async-start | bytes 8388608
  28.3 3.3 %slice-start.2 = ((s8[12582912]{0:T(1024)(128)(4,1)}), s8[4194304]{0:T(1024)(128)(4,1)S(1)}, s32[]{:S(2)}) async-start(s8[12582912]{0:T(1024)(128)(4,1)} %bitcast.91), calls=%async_computation.5 | async-start | bytes 8388608
  31.6 2.1 copy-start.4
  33.7 0.8 copy-start.9
  33.7 2.1 copy-start.11
  101.9 53.3 %copy-start.13 = (bf16[1,2048,512]{2,1,0:T(8,128)(2,1)S(1)}, bf16[1,2048,512]{2,1,0:T(8,128)(2,1)}, u32[]{:S(2)}) copy-start(bf16[1,2048,512]{2,1,0:T(8,128)(2,1)} %param.42) | copy-start | bytes 6291460
  153.8 1.4 copy-start.1
  165.3 3.8 %copy-start.8 = (f32[24,6]{0,1:T(8,128)S(1)}, f32[24,6]{0,1:T(8,128)}, u32[]{:S(2)}) copy-start(f32[24,6]{0,1:T(8,128)} %param.29) | copy-start | bytes 1732
  165.3 5.1 %copy-start.5 = (bf16[2048,256]{1,0:T(8,128)(2,1)S(1)}, bf16[2048,256]{1,0:T(8,128)(2,1)}, u32[]{:S(2)}) copy-start(bf16[2048,256]{1,0:T(8,128)(2,1)} %param.45) | copy-start | bytes 3145732
  165.3 52.5 %all-to-all-start.1 = ((bf16[32,12,2048]{2,1,0:T(8,128)(2,1)}), bf16[32,12,2048]{2,1,0:T(8,128)(2,1)}, u32[]{:S(2)}, u32[]{:S(2)}) async-start(bf16[32,12,2048]{2,1,0:T(8,128)(2,1)} %copy.78), calls=%async_computation.1 | async-start | bytes 4194304 | tf_op jit(solution)/shard_map/all_to_all | solution.py:141
  171.3 52.1 %copy-start.6 = (bf16[256,2048]{1,0:T(8,128)(2,1)S(1)}, bf16[256,2048]{1,0:T(8,128)(2,1)}, u32[]{:S(2)}) copy-start(bf16[256,2048]{1,0:T(8,128)(2,1)} %param.47) | copy-start | bytes 3145732
Sparse Core Ops, SparseCore 0:
  10.9 79.7 all-gather.1
where the time goes:
time: 234 us; the launch traced here: 233 us
  waiting for transfers between devices  102 us (44%)
  blocking collectives  51.9 us (22%)
  matrix products  40.6 us (17%)
  local copies, waits for them, and re-layouts  14.4 us (6%)
  between operations  14.4 us (6%)
  other arithmetic  5.86 us (3%)
  starting transfers between devices  3.82 us (2%)
    all_gather x1, waiting for transfers between devices, shards(): lax.all_gather(w_output, 'ep', axis=1, tiled=True)  54.8 us
    all_to_all x1, blocking collectives, shards(): lax.all_to_all(outgoing, 'ep', split_axis=0, concat_axis=0, tiled=True)  51.9 us
    all_to_all x1, waiting for transfers between devices, shards(): lax.all_to_all(result.reshape(devices * local_experts, count, model), 'ep...  46.5 us
    dot_general x1, matrix products, shards(): jnp.einsum('thl,tkl->thk', query_lat, latent_cache, preferred_element_typ...  8.77 us
    dot_general x1, matrix products, shards(): jnp.dot(values, lax.all_gather(w_output, 'ep', axis=1, tiled=True), prefe...  5.77 us
    dot_general x1, matrix products, shards(): jnp.einsum('sjcf,jfd->sjcd', hidden, expert_down, preferred_element_type=...  5.45 us
  transfers between devices with their start and end apart: 2, of which 2 were waited for; matrix products, arithmetic and copies ran while one was open for 13% of the time, Pallas kernels for 0%

commit v1 on v0

--- a/solution.py
+++ b/solution.py
@@ -106,7 +106,14 @@
     )
     values = values.reshape(rows, model)
     attended = jnp.dot(
-        values, lax.all_gather(w_output, "ep", axis=1, tiled=True), preferred_element_type=f32
+        values,
+        jnp.concatenate(
+            jax.lax.all_to_all(
+                jnp.stack([w_output for _ in range(jax.lax.axis_size("ep"))], 0), "ep", 0, 0
+            ),
+            1,
+        ),
+        preferred_element_type=f32,
     ).astype(bf16)
     residual = (tokens.astype(f32) + attended.astype(f32)).astype(bf16)
     ffn_in = rms_scale(residual.astype(f32), ffn_gain).astype(bf16)

time: 234 us -> 335 us (1.43)
  waiting for transfers between devices: 102 us -> 208 us
  between operations: 14.4 us -> 1.06 us
  starting transfers between devices: 3.82 us -> 11.2 us
  local copies, waits for them, and re-layouts: 14.4 us -> 19.8 us
    all_to_all x0 -> x1, waiting for transfers between devices: none -> 161 us  [shards(): jax.lax.all_to_all(jnp.stack([w_output for _ in range(jax.lax.axis_size('...]
    all_gather x1 -> x0, waiting for transfers between devices: 54.8 us -> none  [shards(): lax.all_gather(w_output, 'ep', axis=1, tiled=True)]
    all_to_all x0 -> x1, starting transfers between devices: none -> 7.46 us  [shards(): jax.lax.all_to_all(jnp.stack([w_output for _ in range(jax.lax.axis_size('...]
    another operation x1 -> x2, local copies, waits for them, and re-layouts: 0.01 us -> 5.38 us  [the longest x1 5.37 us: shards(): jnp.stack([w_output for _ in range(jax.lax.axis_size('ep'))], 0)]
  transfers between devices with their start and end apart: 2 -> 2, of which waited for: 2 -> 2; matrix products, arithmetic and copies ran while one was open for 13% -> 8% of each run, Pallas kernels for 0% -> 0%
where the time goes in v1:
time: 335 us; the launch traced here: 334 us
  waiting for transfers between devices  208 us (62%)
  blocking collectives  51.5 us (15%)
  matrix products  39.2 us (12%)
  local copies, waits for them, and re-layouts  19.8 us (6%)
  starting transfers between devices  11.2 us (3%)
  other arithmetic  3.63 us (1%)
    all_to_all x1, waiting for transfers between devices, shards(): jax.lax.all_to_all(jnp.stack([w_output for _ in range(jax.lax.axis_size('...  161 us
    all_to_all x1, blocking collectives, shards(): lax.all_to_all(outgoing, 'ep', split_axis=0, concat_axis=0, tiled=True)  51.5 us
    all_to_all x1, waiting for transfers between devices, shards(): lax.all_to_all(result.reshape(devices * local_experts, count, model), 'ep...  46.5 us
    dot_general x1, matrix products, shards(): jnp.einsum('thl,tkl->thk', query_lat, latent_cache, preferred_element_typ...  8.47 us
    all_to_all x1, starting transfers between devices, shards(): jax.lax.all_to_all(jnp.stack([w_output for _ in range(jax.lax.axis_size('...  7.46 us
  transfers between devices with their start and end apart: 2, of which 2 were waited for; matrix products, arithmetic and copies ran while one was open for 8% of the time, Pallas kernels for 0%

profile of v1, /device:TPU:0, one launch (start us, length us, event | category | flops | bytes accessed | tf_op | source)
XLA Modules:
  0.0 334.3 jit_solution(18199005317766984877)
XLA Ops:
  0.6 5.4 %stack.2 = bf16[32,2048,64]{1,2,0:T(8,128)(2,1)} broadcast(bf16[2048,64]{0,1:T(8,128)(2,1)} %param.40), dimensions={1,2} | broadcast | bytes 8650752 | tf_op jit(solution)/shard_map/stack | solution.py:112
  6.0 7.5 %all-to-all-start = ((bf16[32,2048,64]{1,2,0:T(8,128)(2,1)}), bf16[32,2048,64]{1,2,0:T(8,128)(2,1)}, u32[]{:S(2)}, u32[]{:S(2)}) async-start(bf16[32,2048,64]{1,2,0:T(8,128)(2,1)} %stack.2), calls=%async_computation | async-start | bytes 16777216 | tf_op jit(solution)/shard_map/all_to_all | solution.py:111
  13.7 1.6 multiply_reduce_fusion.2
  15.8 1.5 convolution_convert_fusion.2
  17.3 0.9 reshape.214
  18.7 1.6 multiply_reduce_fusion.1
  20.5 0.3 fusion.62
  21.0 0.3 fusion.32
  21.3 0.3 copy-done.11
  21.8 8.5 %fusion.50 = f32[24,32,1024]{2,1,0:T(8,128)S(1)} fusion(bf16[24,1024,256]{2,1,0:T(8,128)(2,1)} %param.26, bf16[24,32,256]{2,0,1:T(8,128)(2,1)S(1)} %fusion.32), kind=kOutput, calls=%fused_computation.50 | convolution fusion | flops 402653184 | bytes 16121856 | tf_op jit(solution)/shard_map/thl,tkl->thk/dot_general | solution.py:85
  30.3 2.6 fusion.87
  32.9 0.7 fusion
  33.6 2.1 fusion.28
  35.7 0.5 fusion.33
  36.7 0.6 reduce-window.6
  37.9 161.5 %all-to-all-done = bf16[32,2048,64]{1,2,0:T(8,128)(2,1)} async-done(((bf16[32,2048,64]{1,2,0:T(8,128)(2,1)}), bf16[32,2048,64]{1,2,0:T(8,128)(2,1)}, u32[]{:S(2)}, u32[]{:S(2)}) %all-to-all-start) | async-done | bytes 8388640 | tf_op jit(solution)/shard_map/all_to_all | solution.py:111
  199.4 5.8 %multiply_reduce_fusion = (f32[24]{0:T(128)S(1)}, f32[24,2048]{1,0:T(8,128)S(1)}) fusion(bf16[24,2048]{1,0:T(8,128)(2,1)S(1)} %reshape.216, bf16[2048,2048]{0,1:T(8,128)(2,1)} %bitcast.9, bf16[24,2048]{1,0:T(8,128)(2,1)S(1)} %copy-done.2), kind=kOutput, calls=%fused_computation.64 | convolution fusion | flops 201719776 | bytes 8781920 | tf_op jit(solution)/shard_map/dot_general | solution.py:108
  205.2 1.8 convolution_convert_fusion
  207.0 3.6 %reshape.221 = bf16[32,12,2048]{2,1,0:T(8,128)(2,1)} reshape(bf16[384,2048]{1,0:T(8,128)(2,1)} %convolution_convert_fusion) | data formatting | bytes 3145728 | tf_op jit(solution)/shard_map/reshape | solution.py:137
  210.6 51.5 %all_to_all.15 = bf16[32,12,2048]{2,1,0:T(8,128)(2,1)S(1)} all-to-all(bf16[32,12,2048]{2,1,0:T(8,128)(2,1)} %reshape.221), channel_id=1, replica_groups=mesh['ep'=32] {'ep'}, dimensions={0} | all-to-all | bytes 3145728 | tf_op jit(solution)/shard_map/all_to_all | solution.py:139
  262.1 1.3 copy-done.1
  263.5 1.1 fusion.14
  264.6 5.4 %convolution_convert_fusion.1 = bf16[32,12,2048]{2,0,1:T(8,128)(2,1)} fusion(bf16[1,512,2048]{2,1,0:T(8,128)(2,1)S(1)} %copy-done, bf16[1,2048,512]{2,1,0:T(8,128)(2,1)} %param.43, bf16[32,12,2048]{2,1,0:T(8,128)(2,1)} %copy-done.1, f32[32,1,12,512]{3,0,2,1:T(8,128)S(1)} %fusion.14), kind=kOutput, calls=%fused_computation.4 | convolution fusion | flops 1612578816 | bytes 8126464 | tf_op jit(solution)/shard_map/sjcf,jfd->sjcd/dot_general | solution.py:145
  270.0 3.6 %copy.79 = bf16[32,12,2048]{2,1,0:T(8,128)(2,1)} copy(bf16[32,12,2048]{2,0,1:T(8,128)(2,1)} %convolution_convert_fusion.1) | data formatting | bytes 3145728 | tf_op jit(solution)/shard_map/convert_element_type | solution.py:145
  273.6 3.7 %all-to-all-start.2 = ((bf16[32,12,2048]{2,1,0:T(8,128)(2,1)}), bf16[32,12,2048]{2,1,0:T(8,128)(2,1)}, u32[]{:S(2)}, u32[]{:S(2)}) async-start(bf16[32,12,2048]{2,1,0:T(8,128)(2,1)} %copy.79), calls=%async_computation.2 | async-start | bytes 4194304 | tf_op jit(solution)/shard_map/all_to_all | solution.py:148
  277.4 0.7 pad_maximum_fusion.3
  278.1 0.6 multiply_divide_fusion
  278.7 0.9 fusion.79
  279.6 46.5 %all-to-all-done.2 = bf16[32,12,2048]{2,1,0:T(8,128)(2,1)} async-done(((bf16[32,12,2048]{2,1,0:T(8,128)(2,1)}), bf16[32,12,2048]{2,1,0:T(8,128)(2,1)}, u32[]{:S(2)}, u32[]{:S(2)}) %all-to-all-start.2) | async-done | bytes 1572896 | tf_op jit(solution)/shard_map/all_to_all | solution.py:148
  326.1 3.6 %reshape.235 = bf16[384,2048,1]{1,0,2:T(8,128)(2,1)} reshape(bf16[32,12,2048]{2,1,0:T(8,128)(2,1)} %all-to-all-done.2) | data formatting | bytes 3145728 | tf_op jit(solution)/shard_map/reshape | solution.py:156
  329.7 1.9 fusion.24
  331.6 2.7 fusion.1
  (81 shorter events, 2.8 us)
Async XLA Ops:
  0.6 263.9 %copy-start = (bf16[1,512,2048]{2,1,0:T(8,128)(2,1)S(1)}, bf16[1,512,2048]{2,1,0:T(8,128)(2,1)}, u32[]{:S(2)}) copy-start(bf16[1,512,2048]{2,1,0:T(8,128)(2,1)} %param.44) | copy-start | bytes 6291460
  6.0 7.5 %copy-start.12 = (bf16[2048]{0:T(1024)(128)(2,1)S(1)}, bf16[2048]{0:T(1024)(128)(2,1)}, u32[]{:S(2)}) copy-start(bf16[2048]{0:T(1024)(128)(2,1)} %param.30) | copy-start | bytes 12292
  6.0 7.5 %copy-start.17 = (bf16[256]{0:T(256)(128)(2,1)S(1)}, bf16[256]{0:T(256)(128)(2,1)}, u32[]{:S(2)}) copy-start(bf16[256]{0:T(256)(128)(2,1)} %param.32) | copy-start | bytes 1540
  6.0 7.6 %copy-start.2 = (bf16[24,2048]{1,0:T(8,128)(2,1)S(1)}, bf16[24,2048]{1,0:T(8,128)(2,1)}, u32[]{:S(2)}) copy-start(bf16[24,2048]{1,0:T(8,128)(2,1)} %param.24) | copy-start | bytes 294916
  6.0 9.4 %copy-start.8 = (bf16[256,1024]{1,0:T(8,128)(2,1)S(1)}, bf16[256,1024]{1,0:T(8,128)(2,1)}, u32[]{:S(2)}) copy-start(bf16[256,1024]{1,0:T(8,128)(2,1)} %param.34) | copy-start | bytes 1572868
  6.0 193.4 %all-to-all-start = ((bf16[32,2048,64]{1,2,0:T(8,128)(2,1)}), bf16[32,2048,64]{1,2,0:T(8,128)(2,1)}, u32[]{:S(2)}, u32[]{:S(2)}) async-start(bf16[32,2048,64]{1,2,0:T(8,128)(2,1)} %stack.2), calls=%async_computation | async-start | bytes 16777216 | tf_op jit(solution)/shard_map/all_to_all | solution.py:111
  13.5 2.3 copy-start.14
  13.5 4.7 %copy-start.18 = (bf16[256]{0:T(256)(128)(2,1)S(1)}, bf16[256]{0:T(256)(128)(2,1)}, u32[]{:S(2)}) copy-start(bf16[256]{0:T(256)(128)(2,1)} %param.36) | copy-start | bytes 1540
  13.5 4.7 %copy-start.16 = (bf16[2048,32]{0,1:T(8,128)(2,1)S(1)}, bf16[2048,32]{0,1:T(8,128)(2,1)}, u32[]{:S(2)}) copy-start(bf16[2048,32]{0,1:T(8,128)(2,1)} %param.38) | copy-start | bytes 393220
  18.2 2.8 copy-start.3
  18.2 2.8 copy-start.7
  21.0 0.6 copy-start.11
  21.8 11.8 %slice-start = ((s8[12582912]{0:T(1024)(128)(4,1)}), s8[4194304]{0:T(1024)(128)(4,1)S(1)}, s32[]{:S(2)}) async-start(s8[12582912]{0:T(1024)(128)(4,1)} %bitcast.94), calls=%async_computation.3 | async-start | bytes 8388608
  21.8 11.8 %slice-start.1 = ((s8[12582912]{0:T(1024)(128)(4,1)}), s8[4194304]{0:T(1024)(128)(4,1)S(1)}, s32[]{:S(2)}) async-start(s8[12582912]{0:T(1024)(128)(4,1)} %bitcast.94), calls=%async_computation.4 | async-start | bytes 8388608
  30.3 3.3 slice-start.2
  33.6 2.1 copy-start.4
  35.7 0.8 copy-start.13
  35.7 0.8 copy-start.10
  210.6 52.9 %copy-start.15 = (bf16[1,2048,512]{2,1,0:T(8,128)(2,1)S(1)}, bf16[1,2048,512]{2,1,0:T(8,128)(2,1)}, u32[]{:S(2)}) copy-start(bf16[1,2048,512]{2,1,0:T(8,128)(2,1)} %param.42) | copy-start | bytes 6291460
  262.1 1.4 copy-start.1
  273.6 3.7 %copy-start.9 = (f32[24,6]{0,1:T(8,128)S(1)}, f32[24,6]{0,1:T(8,128)}, u32[]{:S(2)}) copy-start(f32[24,6]{0,1:T(8,128)} %param.29) | copy-start | bytes 1732
  273.6 5.0 %copy-start.5 = (bf16[2048,256]{1,0:T(8,128)(2,1)S(1)}, bf16[2048,256]{1,0:T(8,128)(2,1)}, u32[]{:S(2)}) copy-start(bf16[2048,256]{1,0:T(8,128)(2,1)} %param.45) | copy-start | bytes 3145732
  273.6 52.4 %all-to-all-start.2 = ((bf16[32,12,2048]{2,1,0:T(8,128)(2,1)}), bf16[32,12,2048]{2,1,0:T(8,128)(2,1)}, u32[]{:S(2)}, u32[]{:S(2)}) async-start(bf16[32,12,2048]{2,1,0:T(8,128)(2,1)} %copy.79), calls=%async_computation.2 | async-start | bytes 4194304 | tf_op jit(solution)/shard_map/all_to_all | solution.py:148
  279.6 52.1 %copy-start.6 = (bf16[256,2048]{1,0:T(8,128)(2,1)S(1)}, bf16[256,2048]{1,0:T(8,128)(2,1)}, u32[]{:S(2)}) copy-start(bf16[256,2048]{1,0:T(8,128)(2,1)} %param.47) | copy-start | bytes 3145732
